TPU v7x, 256 devices: a whole 4x4x8 slice. The times are simulated.
256 devices in a mesh: sp: 64 (over z, x, core), tp: 4 (over y).
Axes of the slice: x: 4, y: 4, z: 8, core: 2. Of those that a mesh axis runs over, the one named last changes fastest.
Arguments:
- stream: bfloat16 [16384, 2048], P(('sp', 'tp')), may hold values from -6 to 6
- query_a: bfloat16 [16384, 384], P('sp', 'tp'), may hold values from -400 to 400
- query_b: bfloat16 [16384, 640], P('sp', 'tp'), may hold values from -400 to 400
- latent: bfloat16 [16384, 256], P('sp'), may hold values from -6 to 6
- rotary_key: bfloat16 [16384, 32], P('sp'), may hold values from -6 to 6
- latent_gain: float32 [256], replicated, may hold values from 0.1 to 1.9
- key_gain_a: float32 [96], replicated, may hold values from 0.1 to 1.9
- key_gain_b: float32 [160], replicated, may hold values from 0.1 to 1.9
- w_key_a: bfloat16 [256, 256], P(None, 'tp'), may hold values from -0.375 to 0.375
- w_value_a: bfloat16 [256, 256], P(None, 'tp'), may hold values from -0.375 to 0.375
- w_key_b: bfloat16 [256, 512], P(None, 'tp'), may hold values from -0.375 to 0.375
- w_value_b: bfloat16 [256, 512], P(None, 'tp'), may hold values from -0.375 to 0.375
- w_out_a: bfloat16 [256, 2048], P('tp'), may hold values from -0.21875 to 0.21875
- w_out_b: bfloat16 [512, 2048], P('tp'), may hold values from -0.21875 to 0.21875
- norm_gain: float32 [2048], replicated, may hold values from 0.1 to 1.9
- w_up: bfloat16 [2048, 4096], P('sp', 'tp'), may hold values from -0.125 to 0.125
- w_down: bfloat16 [4096, 2048], P('tp', 'sp'), may hold values from -0.09375 to 0.09375
Outputs:
- result: bfloat16 [16384, 2048], P(('sp', 'tp'))
All inputs are finite; a program needn't handle non-finite values.
Results may differ from a plain program's by a relative error of at most 0.018.
The roundings to bfloat16 on the way count: a program that leaves them out, or rounds other values in their place, can miss the bound.
Values may be sent and summed in bfloat16 or wider, within the bound.
A program may use at most 128 MiB of HBM per device.

v0:
```python
import math

import jax
import jax.numpy as jnp
from jax import lax
from jax.sharding import PartitionSpec as P

NOPE_A = 64
V_A = 64
NOPE_B = 128
V_B = 128
ROPE = 32


EPSILON = 1e-06
THETA = 10000.0


def rows_first(arrays, axis, dims):
    turned = [jnp.moveaxis(a, dim, 0) for a, dim in zip(arrays, dims)]
    widths = [t[0].size for t in turned]
    both = jnp.concatenate([t.reshape(-1, w) for t, w in zip(turned, widths)], axis=1)
    result = lax.all_gather(both, axis, axis=0, tiled=True)
    blocks = jnp.split(result, [sum(widths[:k]) for k in range(1, len(widths))], axis=1)
    return tuple(
        (
            jnp.moveaxis(b.reshape(-1, *t.shape[1:]), 0, dim)
            for b, t, dim in zip(blocks, turned, dims)
        )
    )


def sent_together(arrays, axis, dim, along):
    widths = [a.shape[along] for a in arrays]
    both = jnp.concatenate(arrays, axis=along)
    result = lax.all_gather(both, axis, axis=dim, tiled=True)
    return tuple(jnp.split(result, [sum(widths[:k]) for k in range(1, len(widths))], axis=along))


def cut_along(shard, dim, size):
    lengths = shard.shape
    blocks = shard.reshape(*lengths[:dim], size, lengths[dim] // size, *lengths[dim + 1 :])
    return jnp.moveaxis(blocks, dim, 0)


def summed_on_arrival(shard, axis, dim):
    size = lax.axis_size(axis)
    blocks = lax.all_to_all(cut_along(shard, dim, size), axis, 0, 0, tiled=True)
    return jnp.sum(blocks.astype(jnp.float32), axis=0)


def copy_for_each(shard, axis):
    copies = jnp.broadcast_to(shard, (lax.axis_size(axis), *shard.shape))
    return lax.all_to_all(copies, axis, split_axis=0, concat_axis=0, tiled=True)


def laid_out(blocks, dim):
    blocks = jnp.moveaxis(blocks, 0, dim)
    lengths = blocks.shape
    return blocks.reshape(*lengths[:dim], lengths[dim] * lengths[dim + 1], *lengths[dim + 2 :])


def gathered_copies(shard, axis, dim):
    blocks = copy_for_each(shard, axis)
    return laid_out(blocks, dim)


def rms_scale(values, gain):
    wide = values.astype(jnp.float32)
    return wide * lax.rsqrt(jnp.mean(wide * wide, axis=-1, keepdims=True) + EPSILON) * gain


def rotate(tail, positions):
    half = tail.shape[-1] // 2
    freqs = THETA ** (-jnp.arange(half, dtype=jnp.float32) / half)
    angle = positions[:, None, None] * freqs
    cosine = jnp.cos(angle)
    sine = jnp.sin(angle)
    first = tail[..., :half]
    second = tail[..., half:]
    return jnp.concatenate(
        [first * cosine - second * sine, second * cosine + first * sine], axis=-1
    )


def make_keys(normed, rotary_key, w_key, w_value, key_gain, nope, positions):
    count = normed.shape[0]
    heads = w_key.shape[1] // nope
    head_nope = jnp.dot(normed, w_key, preferred_element_type=jnp.float32).astype(jnp.bfloat16)
    head_nope = head_nope.reshape(count, heads, nope)
    values = jnp.dot(normed, w_value, preferred_element_type=jnp.float32).astype(jnp.bfloat16)
    shared = rotary_key[:, None, :]
    joined = rms_scale(jnp.concatenate([head_nope, shared], axis=-1), key_gain)
    turned = rotate(joined[..., nope:], positions)
    keys_out = jnp.concatenate([joined[..., :nope], turned], axis=-1).astype(jnp.bfloat16)
    return (keys_out.reshape(count, -1), values)


def attend(state, queries, keys_in, values_in, depth):
    maxima, totals, weighted = state
    heads = maxima.shape[1]
    query_view = queries.reshape(queries.shape[0], heads, depth)
    key_view = keys_in.reshape(keys_in.shape[0], heads, depth)
    value_view = values_in.reshape(values_in.shape[0], heads, -1)
    scores = jnp.einsum(
        "qhd,khd->qhk", query_view, key_view, preferred_element_type=jnp.float32
    ) * depth ** (-0.5)
    new_max = jnp.maximum(maxima, jnp.max(scores, axis=-1))
    shifted = jnp.exp(scores - new_max[..., None])
    factor = jnp.exp(maxima - new_max)
    totals = totals * factor + jnp.sum(shifted, axis=-1)
    weighted = weighted * factor[..., None] + jnp.einsum(
        "qhk,khd->qhd", shifted.astype(jnp.bfloat16), value_view, preferred_element_type=jnp.float32
    )
    return (new_max, totals, weighted)


def in_blocks(carry, pieces, step_fn):
    length = pieces[0].shape[0]
    size = math.gcd(length, 1024)
    number = length // size
    stacked = tuple((member.reshape((number, size) + member.shape[1:]) for member in pieces))

    def advance(inner, item):
        position, parts = item
        return (step_fn(inner, parts, position * size), None)

    carry, unused = lax.scan(advance, carry, (jnp.arange(number, dtype=jnp.int32), stacked))
    return carry


def collect(w_up, w_down):
    return rows_first((w_up, w_down), "sp", (0, 1))


def finish(group):
    maxima, totals, weighted = group
    return (weighted / totals[..., None]).astype(jnp.bfloat16).reshape(weighted.shape[0], -1)


def body(
    stream,
    query_a,
    query_b,
    latent,
    rotary_key,
    latent_gain,
    key_gain_a,
    key_gain_b,
    w_key_a,
    w_value_a,
    w_key_b,
    w_value_b,
    w_out_a,
    w_out_b,
    norm_gain,
    w_up,
    w_down,
):
    local = query_a.shape[0]
    depth_a = NOPE_A + ROPE
    depth_b = NOPE_B + ROPE
    heads_a = w_key_a.shape[1] // NOPE_A
    heads_b = w_key_b.shape[1] // NOPE_B

    def empty(heads, width):
        return (
            jnp.full((local, heads), -jnp.inf, jnp.float32),
            jnp.zeros((local, heads), jnp.float32),
            jnp.zeros((local, heads, width), jnp.float32),
        )

    start_state = (empty(heads_a, V_A), empty(heads_b, V_B))

    def attend_both(state, keys_a, values_a, keys_b, values_b):
        return (
            attend(state[0], query_a, keys_a, values_a, depth_a),
            attend(state[1], query_b, keys_b, values_b, depth_b),
        )

    positions = (lax.axis_index("sp") * local + jnp.arange(local, dtype=jnp.int32)).astype(
        jnp.float32
    )
    normed_latent = rms_scale(latent, latent_gain).astype(jnp.bfloat16)
    own_keys_a, own_values_a = make_keys(
        normed_latent, rotary_key, w_key_a, w_value_a, key_gain_a, NOPE_A, positions
    )
    own_keys_b, own_values_b = make_keys(
        normed_latent, rotary_key, w_key_b, w_value_b, key_gain_b, NOPE_B, positions
    )

    def from_keys(state, pieces, start):
        return attend_both(state, pieces[0], pieces[1], pieces[2], pieces[3])

    state = in_blocks(
        start_state,
        sent_together((own_keys_a, own_values_a, own_keys_b, own_values_b), "sp", 0, 1),
        from_keys,
    )
    attended_a = finish(state[0])
    attended_b = finish(state[1])
    mixed = summed_on_arrival(
        (
            jnp.dot(attended_a, w_out_a, preferred_element_type=jnp.float32)
            + jnp.dot(attended_b, w_out_b, preferred_element_type=jnp.float32)
        ).astype(jnp.bfloat16),
        "tp",
        0,
    )
    residual = (stream.astype(jnp.float32) + mixed).astype(jnp.bfloat16)
    normed = rms_scale(residual, norm_gain).astype(jnp.bfloat16)
    up_full, down_full = collect(w_up, w_down)
    hidden = jnp.dot(gathered_copies(normed, "tp", 0), up_full, preferred_element_type=jnp.float32)
    activated = jnp.square(jax.nn.relu(hidden)).astype(jnp.bfloat16)
    summed = summed_on_arrival(
        jnp.dot(activated, down_full, preferred_element_type=jnp.float32).astype(jnp.bfloat16),
        "tp",
        0,
    )
    return (residual.astype(jnp.float32) + summed).astype(jnp.bfloat16)


def solution(mesh):
    in_specs = (
        P(("sp", "tp"), None),
        P("sp", "tp"),
        P("sp", "tp"),
        P("sp", None),
        P("sp", None),
        P(),
        P(),
        P(),
        P(None, "tp"),
        P(None, "tp"),
        P(None, "tp"),
        P(None, "tp"),
        P("tp", None),
        P("tp", None),
        P(),
        P("sp", "tp"),
        P("tp", "sp"),
    )
    out_specs = P(("sp", "tp"), None)
    return jax.shard_map(body, mesh=mesh, in_specs=in_specs, out_specs=out_specs, check_vma=False)
```

profile of v0, /device:TPU:1, one launch (start us, length us, event | category | flops | bytes accessed | tf_op | source)
XLA Modules:
  0.0 319.7 jit_solution(17929350222609711373)
XLA Ops:
  17.0 1.5 pad_maximum_fusion
  18.6 102.6 %all-gather.3.cloned.1.call-done = bf16[16384,448]{0,1:T(8,128)(2,1)} async-done(((bf16[256,448]{0,1:T(8,128)(2,1)}), bf16[16384,448]{0,1:T(8,128)(2,1)}) %all-gather.3.cloned.1.call-update) | async-done | bytes 14680080 | tf_op jit(solution)/shard_map/all_gather | solution.py:36
  121.2 5.2 %split.26 = bf16[16384,160]{0,1:T(8,128)(2,1)} slice(bf16[16384,448]{0,1:T(8,128)(2,1)} %all-gather.3.cloned.1.call-done), slice={[0:16384], [160:320]} | slice | bytes 10485760 | tf_op jit(solution)/shard_map/split | solution.py:37
  126.4 9.7 %copy.24 = bf16[16384,160]{1,0:T(8,128)(2,1)} copy(bf16[16384,160]{0,1:T(8,128)(2,1)} %split.26) | data formatting | bytes 10485760
  136.2 4.6 %split.27 = bf16[16384,128]{0,1:T(8,128)(2,1)} slice(bf16[16384,448]{0,1:T(8,128)(2,1)} %all-gather.3.cloned.1.call-done), slice={[0:16384], [320:448]} | slice | bytes 8388608 | tf_op jit(solution)/shard_map/split | solution.py:37
  140.7 6.4 %copy.25 = bf16[16384,128]{1,0:T(8,128)(2,1)} copy(bf16[16384,128]{0,1:T(8,128)(2,1)} %split.27) | data formatting | bytes 8388608
  147.1 3.8 %split.24 = bf16[16384,96]{0,1:T(8,128)(2,1)} slice(bf16[16384,448]{0,1:T(8,128)(2,1)} %all-gather.3.cloned.1.call-done), slice={[0:16384], [0:96]} | slice | bytes 6291456 | tf_op jit(solution)/shard_map/split | solution.py:37
  150.9 6.0 %copy.22 = bf16[16384,96]{1,0:T(8,128)(2,1)} copy(bf16[16384,96]{0,1:T(8,128)(2,1)} %split.24) | data formatting | bytes 6291456
  156.9 3.2 copy.23
  160.1 92.5 %while.21 = (s32[]{:T(128)}, f32[256,1]{0,1:T(1,128)S(1)}, f32[256,1]{0,1:T(1,128)S(1)}, f32[256,1,64]{0,2,1:T(8,128)S(1)}, f32[256,1]{0,1:T(1,128)S(1)}, /*inde...) while((s32[]{:T(128)}, f32[256,1]{0,1:T(1,128)S(1)}, ...), condition=%wide.region_8.9_spmd.clone, body=%wide.region_3.8_spmd.clone.sunk | while | flops 238176768 | bytes 8161435 | solution.py:128
  160.1 1.4 fusion.130
  161.8 1.3 fusion.127
  163.3 1.3 fusion.135
  165.9 1.4 fusion.130
  167.6 1.3 fusion.127
  169.1 1.3 fusion.135
  171.7 1.4 fusion.130
  173.3 1.3 fusion.127
  174.9 1.3 fusion.135
  177.5 1.5 fusion.130
  179.2 1.3 fusion.127
  180.7 1.3 fusion.135
  182.0 1.3 fusion.134
  183.3 1.4 fusion.130
  186.5 1.3 fusion.135
  187.8 1.3 fusion.134
  189.2 1.4 fusion.130
  192.3 1.3 fusion.135
  193.6 1.3 fusion.134
  194.9 1.4 fusion.130
  196.6 1.3 fusion.127
  198.1 1.3 fusion.135
  200.7 1.4 fusion.130
  202.4 1.3 fusion.127
  203.9 1.3 fusion.135
  206.5 1.4 fusion.130
  208.1 1.3 fusion.127
  209.7 1.3 fusion.135
  212.3 1.4 fusion.130
  213.9 1.3 fusion.127
  215.4 1.3 fusion.135
  218.0 1.4 fusion.130
  219.7 1.3 fusion.127
  221.2 1.3 fusion.135
  223.8 1.4 fusion.130
  225.4 1.3 fusion.127
  227.0 1.3 fusion.135
  229.6 1.4 fusion.130
  231.2 1.3 fusion.127
  232.7 1.3 fusion.135
  235.3 1.4 fusion.130
  237.0 1.3 fusion.127
  238.5 1.3 fusion.135
  241.1 1.4 fusion.130
  242.7 1.3 fusion.127
  244.3 1.3 fusion.135
  246.9 1.4 fusion.130
  248.5 1.3 fusion.127
  250.0 1.3 fusion.135
  253.6 18.5 %all_to_all.15 = bf16[4,64,2048]{2,1,0:T(8,128)(2,1)S(1)} all-to-all(bf16[4,64,2048]{2,1,0:T(8,128)(2,1)S(1)} %bitcast.162), channel_id=1, replica_groups=mesh['sp'=64,'tp'=4] {'tp'}, dimensions={0} | all-to-all | bytes 2097152 | tf_op jit(solution)/shard_map/all_to_all | solution.py:48
  273.7 3.5 %all-to-all-start.1 = ((bf16[4,64,2048]{2,1,0:T(8,128)(2,1)}), bf16[4,64,2048]{2,1,0:T(8,128)(2,1)S(1)}, u32[]{:S(2)}, u32[]{:S(2)}) async-start(bf16[4,64,2048]{2,1,0:T(8,128)(2,1)} %broadcast_in_dim.8), calls=%async_computation.1 | async-start | bytes 2097152 | tf_op jit(solution)/shard_map/all_to_all | solution.py:54
  277.2 13.8 %all-to-all-done.1 = bf16[4,64,2048]{2,1,0:T(8,128)(2,1)S(1)} async-done(((bf16[4,64,2048]{2,1,0:T(8,128)(2,1)}), bf16[4,64,2048]{2,1,0:T(8,128)(2,1)S(1)}, u32[]{:S(2)}, u32[]{:S(2)}) %all-to-all-start.1) | async-done | bytes 1048608 | tf_op jit(solution)/shard_map/all_to_all | solution.py:54
  291.0 5.8 %fusion.37 = bf16[256,2048]{1,0:T(8,128)(2,1)S(1)} fusion(bf16[2048,2048]{1,0:T(8,128)(2,1)} %all-gather.5.cloned.1.call-done, bf16[256,2048]{1,0:T(8,128)(2,1)S(1)} %bitcast.163), kind=kOutput, calls=%fused_computation.50 | convolution fusion | flops 2148794368 | bytes 10485760 | tf_op jit(solution)/shard_map/dot_general | solution.py:216
  296.8 15.1 %all_to_all.16 = bf16[4,64,2048]{2,1,0:T(8,128)(2,1)S(1)} all-to-all(bf16[4,64,2048]{2,1,0:T(8,128)(2,1)S(1)} %bitcast.164), channel_id=1, replica_groups=mesh['sp'=64,'tp'=4] {'tp'}, dimensions={0} | all-to-all | bytes 2097152 | tf_op jit(solution)/shard_map/all_to_all | solution.py:48
  (183 shorter events, 40.6 us)
Async XLA Ops:
  6.5 246.1 %copy-start = (bf16[128,2048]{1,0:T(8,128)(2,1)S(1)}, bf16[128,2048]{1,0:T(8,128)(2,1)}, u32[]{:S(2)}) copy-start(bf16[128,2048]{1,0:T(8,128)(2,1)} %param.32) | copy-start | bytes 1572868
  6.5 114.7 %all-gather.3.cloned.1.call-start = ((), (), s32[]{:S(2)}) async-start(), calls=%async_computation.3 | async-start | bytes 14909440 | tf_op jit(solution)/shard_map/all_gather | solution.py:36
  16.2 0.7 copy-start.3
  16.9 260.3 %all-gather.5.cloned.1.call-start = ((), (), s32[]{:S(2)}) async-start(), calls=%async_computation.4 | async-start | bytes 8519680 | tf_op jit(solution)/shard_map/all_gather | solution.py:23
  150.9 6.0 %slice-start = ((bf16[16384,448]{0,1:T(8,128)(2,1)}), bf16[16384,64]{0,1:T(8,128)(2,1)S(1)}, s32[]{:S(2)}) async-start(bf16[16384,448]{0,1:T(8,128)(2,1)} %all-gather.3.cloned.1.call-done), calls=%async_computation.5 | async-start | bytes 4194304 | tf_op jit(solution)/shard_map/split | solution.py:37
  156.9 3.2 copy-start.1
  156.9 3.2 copy-start.2
  160.1 93.0 %copy-start.4 = (bf16[64,2048]{1,0:T(8,128)(2,1)S(1)}, bf16[64,2048]{1,0:T(8,128)(2,1)}, u32[]{:S(2)}) copy-start(bf16[64,2048]{1,0:T(8,128)(2,1)} %param.31) | copy-start | bytes 786436
  253.1 19.1 %copy-start.5 = (bf16[64,2048]{1,0:T(8,128)(2,1)S(1)}, bf16[64,2048]{1,0:T(8,128)(2,1)}, u32[]{:S(2)}) copy-start(bf16[64,2048]{1,0:T(8,128)(2,1)} %param.19) | copy-start | bytes 786436
  253.1 19.3 %copy-start.6 = (f32[2048]{0:T(1024)S(1)}, f32[2048]{0:T(1024)}, u32[]{:S(2)}) copy-start(f32[2048]{0:T(1024)} %param.33) | copy-start | bytes 24580
  273.7 17.3 %all-to-all-start.1 = ((bf16[4,64,2048]{2,1,0:T(8,128)(2,1)}), bf16[4,64,2048]{2,1,0:T(8,128)(2,1)S(1)}, u32[]{:S(2)}, u32[]{:S(2)}) async-start(bf16[4,64,2048]{2,1,0:T(8,128)(2,1)} %broadcast_in_dim.8), calls=%async_computation.1 | async-start | bytes 2097152 | tf_op jit(solution)/shard_map/all_to_all | solution.py:54
Sparse Core Ops, SparseCore 0:
  17.1 104.0 all-gather.2
  124.0 82.8 all-gather.4
where the time goes:
time: 326 us; the launch traced here: 320 us
  waiting for transfers between devices  116 us (36%)
  matrix products  95.2 us (29%)
  local copies, waits for them, and re-layouts  40.8 us (13%)
  blocking collectives  33.6 us (10%)
  other arithmetic  15.4 us (5%)
  between operations  13.6 us (4%)
  starting transfers between devices  3.56 us (1%)
    all_gather x1, waiting for transfers between devices, sent_together(): result = lax.all_gather(both, axis, axis=dim, tiled=True)  103 us
    dot_general x32, matrix products, attend(): jnp.einsum('qhd,khd->qhk', query_view, key_view, preferred_element_type=j...  42.6 us
    dot_general x32, matrix products, attend(): jnp.einsum('qhk,khd->qhd', shifted.astype(jnp.bfloat16), value_view, pref...  41.2 us
    all_to_all x2, blocking collectives, summed_on_arrival(): blocks = lax.all_to_all(cut_along(shard, dim, size), axis, 0, 0, tiled=True)  33.6 us
    unnamed x20, local copies, waits for them, and re-layouts  26 us
    all_to_all x1, waiting for transfers between devices, copy_for_each(): return lax.all_to_all(copies, axis, split_axis=0, concat_axis=0, tiled=True)  13.8 us
    split x5, local copies, waits for them, and re-layouts, sent_together(): jnp.split(result, [sum(widths[:k]) for k in range(1, len(widths))], axis=...  13.6 us
    reduce_sum x32, other arithmetic, attend(): totals = totals * factor + jnp.sum(shifted, axis=-1)  7.12 us
  transfers between devices with their start and end apart: 3, of which 2 were waited for; matrix products, arithmetic and copies ran while one was open for 42% of the time, Pallas kernels for 0%

commit v1 on v0

v1 whole, which is shorter than its diff:
```python
import functools
import math

import jax
import jax.numpy as jnp
from jax import lax
from jax.experimental import pallas as pl
from jax.experimental.pallas import tpu as pltpu
from jax.sharding import PartitionSpec as P

NOPE_A = 64
V_A = 64
NOPE_B = 128
V_B = 128
ROPE = 32
DEPTH_A = NOPE_A + ROPE
DEPTH_B = NOPE_B + ROPE
KV = NOPE_A + NOPE_B + V_A + V_B
OUT = V_A + V_B
RANK = 256
D = 2048
FF = 1024
TOK = 256
OWN = 64
Z, X, C, Y = 8, 4, 2, 4
EPSILON = 1e-06
THETA = 10000.0
LOG2E = 1.4426950408889634
SCALE_A = DEPTH_A ** (-0.5) * LOG2E
SCALE_B = DEPTH_B ** (-0.5) * LOG2E
NT = (((1,), (1,)), ((), ()))
NN = (((1,), (0,)), ((), ()))
F32 = jnp.float32
BF16 = jnp.bfloat16


def mm(a, b, dims):
    return lax.dot_general(a, b, dims, preferred_element_type=F32)


def kernel(
    lat_in,
    q_in,
    up_in,
    dn_in,
    woa_in,
    wob_in,
    st_in,
    wt,
    lgain,
    kgain,
    ngain,
    trig,
    out,
    lat,
    qb,
    up,
    dn,
    wo,
    st,
    kta,
    ktb,
    ka,
    kb,
    va,
    vb,
    oacc,
    stat,
    osend,
    orecv,
    srecv,
    att,
    res,
    nrm,
    act,
    pb,
    rb,
    loc,
    lat_s,
    lat_r,
    latp_s,
    latp_r,
    q_s,
    q_r,
    upx_s,
    upx_r,
    upz_s,
    upz_r,
    upp_s,
    upp_r,
    dnz_s,
    dnz_r,
    dnx_s,
    dnx_r,
    dnp_s,
    dnp_r,
    st_s,
    st_r,
    wo_s,
    wo_r,
    wop_s,
    wop_r,
    ox_s,
    ox_r,
    sx_s,
    sx_r,
    ay_s,
    ay_r,
    rs_s,
    rs_r,
):
    sp = lax.axis_index("sp")
    y = lax.axis_index("tp")
    z = lax.div(sp, 8)
    x = lax.rem(lax.div(sp, 2), 4)
    c = lax.rem(sp, 2)
    oc = 1 - c

    def wrap(v, n):
        return lax.rem(v + 2 * n, n)

    def dev(z_, x_, c_, y_):
        return {"sp": z_ * 8 + x_ * 2 + c_, "tp": y_}

    partner = dev(z, x, oc, y)
    zdev = (dev(wrap(z + 1, Z), x, c, y), dev(wrap(z - 1, Z), x, c, y))
    xdev = [None] + [dev(z, wrap(x + d, X), c, y) for d in (1, 2, 3)]
    ydev = [None] + [dev(z, x, c, wrap(y + d, Y)) for d in (1, 2, 3)]

    def rdma(src, dst, ss, rs, where):
        return pltpu.make_async_remote_copy(
            src_ref=src,
            dst_ref=dst,
            send_sem=ss,
            recv_sem=rs,
            device_id=where,
            device_id_type=pl.DeviceIdType.MESH,
        )

    def same(ref, ss, rs, where):
        return rdma(ref, ref, ss, rs, where)

    locals_ = [
        pltpu.make_async_copy(lat_in, lat.at[z, c], loc.at[0]),
        pltpu.make_async_copy(q_in, qb.at[x], loc.at[1]),
        pltpu.make_async_copy(up_in, up.at[z, x, c], loc.at[2]),
        pltpu.make_async_copy(dn_in, dn.at[z, x, c], loc.at[3]),
        pltpu.make_async_copy(st_in, st.at[y], loc.at[4]),
        pltpu.make_async_copy(woa_in, wo.at[y, pl.ds(0, V_A)], loc.at[5]),
        pltpu.make_async_copy(wob_in, wo.at[y, pl.ds(V_A, V_B)], loc.at[6]),
    ]
    for cp in locals_:
        cp.start()

    barrier = pltpu.get_barrier_semaphore()
    for where in [partner, *zdev, *xdev[1:], *ydev[1:]]:
        pl.semaphore_signal(
            barrier, inc=1, device_id=where, device_id_type=pl.DeviceIdType.MESH
        )

    kta[...] = jnp.zeros_like(kta)
    ktb[...] = jnp.zeros_like(ktb)
    oacc[...] = jnp.zeros_like(oacc)
    for j in range(X):
        stat[j] = jnp.zeros((8, TOK), F32)
        stat[j, 0:1] = jnp.full((1, TOK), -jnp.inf, F32)
        stat[j, 2:3] = jnp.full((1, TOK), -jnp.inf, F32)

    def lat_ring(way, s, zsrc):
        return same(lat.at[zsrc, c], lat_s.at[way, s], lat_r.at[way, s], zdev[way])

    def lat_part(way, s, zsrc):
        return same(lat.at[zsrc, c], latp_s.at[way, s], latp_r.at[way, s], partner)

    def q_x(d):
        return same(qb.at[x], q_s.at[d - 1], q_r.at[d - 1], xdev[d])

    def up_x(d):
        return same(up.at[z, x, c], upx_s.at[d - 1], upx_r.at[d - 1], xdev[d])

    def up_ring(way, s, zsrc):
        return same(up.at[zsrc, :, c], upz_s.at[way, s], upz_r.at[way, s], zdev[way])

    def up_part(way, s, zsrc):
        return same(up.at[zsrc, :, c], upp_s.at[way, s], upp_r.at[way, s], partner)

    def dn_ring(way, s, zsrc):
        return same(dn.at[zsrc, x, c], dnz_s.at[way, s], dnz_r.at[way, s], zdev[way])

    def dn_x(d, zsrc):
        return same(dn.at[zsrc, x, c], dnx_s.at[d - 1], dnx_r.at[d - 1], xdev[d])

    def dn_x_all(d):
        return same(dn.at[:, wrap(x - d, X), c], dnx_s.at[d - 1], dnx_r.at[d - 1], xdev[d])

    def dn_part(d):
        return same(dn.at[:, wrap(x - d, X), c], dnp_s.at[d], dnp_r.at[d], partner)

    def st_y(d):
        return same(st.at[y], st_s.at[d - 1], st_r.at[d - 1], ydev[d])

    half = pl.ds(pl.multiple_of(c * (D // 2), D // 2), D // 2)

    def wo_y(d):
        return same(wo.at[y, :, half], wo_s.at[d - 1], wo_r.at[d - 1], ydev[d])

    def wo_part(d):
        return same(
            wo.at[wrap(y - d, Y), :, half], wop_s.at[d - 1], wop_r.at[d - 1], partner
        )

    def o_x(d):
        return rdma(
            osend.at[wrap(x + d, X)], orecv.at[x], ox_s.at[d - 1], ox_r.at[d - 1], xdev[d]
        )

    def s_x(d):
        return rdma(
            stat.at[wrap(x + d, X)], srecv.at[x], sx_s.at[d - 1], sx_r.at[d - 1], xdev[d]
        )

    def a_y(d):
        return same(att.at[y], ay_s.at[d - 1], ay_r.at[d - 1], ydev[d])

    def r_y(d, n):
        return rdma(
            pb.at[n, wrap(y + d, Y)],
            rb.at[y, n],
            rs_s.at[d - 1, n],
            rs_r.at[d - 1, n],
            ydev[d],
        )

    for cp in locals_:
        cp.wait()
    pl.semaphore_wait(barrier, 9)

    lat_ring(0, 1, z).start()
    lat_ring(1, 1, z).start()
    lat_part(0, 0, z).start()
    for d in (2, 1, 3):
        q_x(d).start()
    for way in (0, 1):
        dn_ring(way, 1, z).start()
    for d in (2, 1, 3):
        up_x(d).start()
    for d in (2, 1, 3):
        dn_x(d, z).start()
    for d in (2, 1, 3):
        st_y(d).start()
    for d in (2, 1, 3):
        wo_y(d).start()

    def prep(zi, ci, i):
        rows = pl.ds(i * TOK, TOK)
        raw = lat[zi, ci, pl.ds(0, TOK), :].astype(F32)
        mean = jnp.mean(raw * raw, axis=-1, keepdims=True)
        nl = (raw * lax.rsqrt(mean + EPSILON) * lgain[...]).astype(BF16)
        kv = mm(wt[...], nl, NT).astype(BF16)
        va[:, rows] = kv[NOPE_A + NOPE_B : NOPE_A + NOPE_B + V_A]
        vb[:, rows] = kv[NOPE_A + NOPE_B + V_A :]
        rope = lat[zi, ci, pl.ds(TOK, ROPE), :].astype(F32)
        slot = zi * 2 + ci
        cosine = trig[slot, 0:16]
        sine = trig[slot, 16:32]
        square = jnp.sum(rope * rope, axis=0, keepdims=True)

        def one_head(nope, depth, base, dst):
            width = depth - ROPE
            wide = nope.astype(F32)
            total = jnp.sum(wide * wide, axis=0, keepdims=True) + square
            r = lax.rsqrt(total * (1.0 / depth) + EPSILON)
            dst[pl.ds(base, width), :] = (
                wide * r * kgain[pl.ds(base, width), :]
            ).astype(BF16)
            tail = rope * r * kgain[pl.ds(base + width, ROPE), :]
            first = tail[0:16]
            second = tail[16:32]
            dst[pl.ds(base + width, 16), :] = (first * cosine - second * sine).astype(BF16)
            dst[pl.ds(base + width + 16, 16), :] = (
                second * cosine + first * sine
            ).astype(BF16)

        one_head(kv[0:NOPE_A], DEPTH_A, 0, kta)
        one_head(kv[NOPE_A : NOPE_A + NOPE_B], DEPTH_B, DEPTH_A, ktb)
        ka[rows, :] = kta[...].T
        kb[rows, :] = ktb[...].T

    def attend(j, carry):
        queries = qb[j]
        for keys, values, row, scale, lo, width in (
            (ka, va, 0, SCALE_A, 0, V_A),
            (kb, vb, 2, SCALE_B, V_A, V_B),
        ):
            scores = mm(keys[...], queries, NT) * scale
            old = stat[j, row : row + 1]
            new = jnp.maximum(old, jnp.max(scores, axis=0, keepdims=True))
            factor = jnp.exp2(old - new)
            shifted = jnp.exp2(scores - new)
            stat[j, row : row + 1] = new
            stat[j, row + 1 : row + 2] = stat[j, row + 1 : row + 2] * factor + jnp.sum(
                shifted, axis=0, keepdims=True
            )
            part = mm(values[...], shifted.astype(BF16), NN)
            oacc[j, pl.ds(lo, width), :] = oacc[j, pl.ds(lo, width), :] * factor + part
        return carry

    def unit(t, carry):
        odd = lax.rem(t, 2)
        s = lax.div(t + 1, 2)
        edge = lax.div(t, 7) + lax.div(7 - t, 7)
        zm = wrap(z - s, Z)
        zp = wrap(z + s, Z)

        @pl.when(odd == 1)
        def _():
            lat_ring(0, s, zm).wait_recv()

            @pl.when(s < 4)
            def _():
                lat_ring(0, s + 1, zm).start()
                lat_ring(1, s, zp).wait_recv()

                @pl.when(s < 3)
                def _():
                    lat_ring(1, s + 1, zp).start()

                lat_part(1, s, zp).start()

            lat_part(0, s, zm).start()

            dn_ring(0, s, zm).wait_recv()

            @pl.when(s < 4)
            def _():
                dn_ring(0, s + 1, zm).start()
                dn_ring(1, s, zp).wait_recv()

                @pl.when(s < 3)
                def _():
                    dn_ring(1, s + 1, zp).start()

                for d in (2, 1, 3):
                    dn_x(d, zp).start()

            for d in (2, 1, 3):
                dn_x(d, zm).start()

            @pl.when(s == 1)
            def _():
                for d in (1, 2, 3):
                    up_x(d).wait_recv()
                up_ring(0, 1, z).start()
                up_ring(1, 1, z).start()
                up_part(0, 0, z).start()

            @pl.when(s > 1)
            def _():
                su = s - 1
                um = wrap(z - su, Z)
                un = wrap(z + su, Z)
                up_ring(1, su, un).wait_recv()
                up_ring(1, su + 1, un).start()
                up_ring(0, su, um).wait_recv()

                @pl.when(su < 3)
                def _():
                    up_ring(0, su + 1, um).start()

                up_part(0, su, um).start()
                up_part(1, su, un).start()

        @pl.when((odd == 0) | (t == 7))
        def _():
            lat_part(0, s, zm).wait_recv()

        @pl.when((odd == 0) & (t > 0))
        def _():
            lat_part(1, s, zp).wait_recv()

        flip_a = (1 - odd) * (1 - edge)
        flip_b = 1 - odd * (1 - edge)
        prep(zm, c + flip_a * (1 - 2 * c), 0)
        prep(wrap(z + s - 2 * s * edge, Z), c + flip_b * (1 - 2 * c), 1)

        @pl.when(t == 0)
        def _():
            for d in (1, 2, 3):
                q_x(d).wait_recv()

        lax.fori_loop(0, X, attend, 0)
        return carry

    lax.fori_loop(0, 8, unit, 0)

    for j in range(X):
        osend[j, 0:V_A] = (oacc[j, 0:V_A] / stat[j, 1:2]).astype(BF16)
        osend[j, V_A:OUT] = (oacc[j, V_A:OUT] / stat[j, 3:4]).astype(BF16)
    for d in (2, 1, 3):
        s_x(d).start()
        o_x(d).start()
    orecv[x] = osend[x]
    srecv[x] = stat[x]

    up_ring(1, 4, wrap(z + 4, Z)).wait_recv()
    up_part(1, 4, wrap(z + 4, Z)).start()
    dn_part(0).start()
    for d in (1, 2, 3):
        wo_y(d).wait_recv()
        wo_part(d).start()

    for d in (1, 2, 3):
        s_x(d).wait_recv()
        o_x(d).wait_recv()

    for row, lo, width in ((0, 0, V_A), (2, V_A, V_B)):
        peaks = [srecv[i, row : row + 1] for i in range(X)]
        top = functools.reduce(jnp.maximum, peaks)
        shares = [srecv[i, row + 1 : row + 2] * jnp.exp2(peaks[i] - top) for i in range(X)]
        total = shares[0] + shares[1] + shares[2] + shares[3]
        mixed = orecv[0, lo : lo + width].astype(F32) * shares[0]
        for i in range(1, X):
            mixed = mixed + orecv[i, lo : lo + width].astype(F32) * shares[i]
        att[y, pl.ds(lo, width), :] = (mixed / total).astype(BF16)
    for d in (2, 1, 3):
        a_y(d).start()

    for d in (1, 2, 3):
        dn_x_all(d).wait_recv()
        dn_part(d).start()
    for d in (1, 2, 3):
        st_y(d).wait_recv()
        wo_part(d).wait_recv()
    for d in (1, 2, 3):
        a_y(d).wait_recv()

    attended = att[...].reshape(Y * OUT, TOK).T
    squares = jnp.zeros((TOK, 1), F32)
    for n in range(4):
        cols = slice(n * 512, n * 512 + 512)
        weights = wo[:, :, cols].reshape(Y * OUT, 512)
        mixed = mm(attended, weights, NN)
        summed = (st[:, :, cols].reshape(TOK, 512).astype(F32) + mixed).astype(BF16)
        res[:, cols] = summed
        wide = summed.astype(F32)
        squares = squares + jnp.sum(wide * wide, axis=-1, keepdims=True)
    r = lax.rsqrt(squares * (1.0 / D) + EPSILON)
    for n in range(4):
        cols = slice(n * 512, n * 512 + 512)
        nrm[:, cols] = (res[:, cols].astype(F32) * r * ngain[:, cols]).astype(BF16)

    up_part(0, 0, z).wait_recv()
    for s in (1, 2, 3):
        up_part(0, s, z).wait_recv()
    for s in (1, 2, 3, 4):
        up_part(1, s, z).wait_recv()

    for n in range(4):
        cols = slice(n * 256, n * 256 + 256)
        hidden = jnp.maximum(mm(nrm[...], up[:, :, :, :, cols].reshape(D, 256), NN), 0.0)
        act[:, cols] = (hidden * hidden).astype(BF16)

    for d in (0, 1, 2, 3):
        dn_part(d).wait_recv()

    for n in range(4):
        weights = dn[2 * n : 2 * n + 2].reshape(512, FF)
        part = mm(act[...], weights, NT).astype(BF16)
        pb[n] = part.reshape(Y, OWN, 512)
        for d in (2, 1, 3):
            r_y(d, n).start()

    mine = pl.ds(pl.multiple_of(y * OWN, OWN), OWN)
    for n in range(4):
        cols = slice(n * 512, n * 512 + 512)
        total = pb[n, y].astype(F32)
        for d in (1, 2, 3):
            r_y(d, n).wait_recv()
            total = total + rb[wrap(y - d, Y), n].astype(F32)
        out[:, cols] = (res[mine, cols].astype(F32) + total).astype(BF16)

    lat_part(0, 0, z).wait_send()
    up_part(0, 0, z).wait_send()
    for s in (1, 2, 3, 4):
        lat_ring(0, s, z).wait_send()
        lat_part(0, s, z).wait_send()
        dn_ring(0, s, z).wait_send()
        up_ring(1, s, z).wait_send()
        up_part(1, s, z).wait_send()
    for s in (1, 2, 3):
        lat_ring(1, s, z).wait_send()
        lat_part(1, s, z).wait_send()
        dn_ring(1, s, z).wait_send()
        up_ring(0, s, z).wait_send()
        up_part(0, s, z).wait_send()
    for d in (1, 2, 3):
        q_x(d).wait_send()
        up_x(d).wait_send()
        dn_x_all(d).wait_send()
        st_y(d).wait_send()
        wo_y(d).wait_send()
        wo_part(d).wait_send()
        o_x(d).wait_send()
        s_x(d).wait_send()
        a_y(d).wait_send()
        for n in range(4):
            r_y(d, n).wait_send()
    for d in (0, 1, 2, 3):
        dn_part(d).wait_send()


def body(
    stream,
    query_a,
    query_b,
    latent,
    rotary_key,
    latent_gain,
    key_gain_a,
    key_gain_b,
    w_key_a,
    w_value_a,
    w_key_b,
    w_value_b,
    w_out_a,
    w_out_b,
    norm_gain,
    w_up,
    w_down,
):
    sp = lax.axis_index("sp")
    x = (sp // 2) % X
    queries = jnp.concatenate([query_a, query_b], axis=1)
    packed = jnp.concatenate([latent, rotary_key.T], axis=0)
    wt = jnp.concatenate([w_key_a, w_key_b, w_value_a, w_value_b], axis=1).T
    gains = jnp.broadcast_to(
        jnp.concatenate([key_gain_a, key_gain_b])[:, None], (DEPTH_A + DEPTH_B, TOK)
    )
    chunk = jnp.arange(Z, dtype=jnp.int32)[:, None] * 8 + x * 2 + jnp.arange(C, dtype=jnp.int32)
    positions = chunk.reshape(-1, 1) * TOK + jnp.arange(TOK, dtype=jnp.int32)
    freqs = THETA ** (-jnp.arange(ROPE // 2, dtype=F32) / (ROPE // 2))
    angle = positions.astype(F32)[:, None, :] * freqs[:, None]
    trig = jnp.concatenate([jnp.cos(angle), jnp.sin(angle)], axis=1)

    hbm = pl.BlockSpec(memory_space=pltpu.HBM)
    vmem = pl.BlockSpec(memory_space=pltpu.VMEM)
    dma = pltpu.SemaphoreType.DMA
    return pl.pallas_call(
        kernel,
        out_shape=jax.ShapeDtypeStruct((OWN, D), BF16),
        in_specs=[hbm] * 7 + [vmem] * 5,
        out_specs=vmem,
        scratch_shapes=[
            pltpu.VMEM((Z, C, TOK + ROPE, RANK), BF16),
            pltpu.VMEM((X, TOK, DEPTH_A + DEPTH_B), BF16),
            pltpu.VMEM((Z, X, C, 32, FF), BF16),
            pltpu.VMEM((Z, X, C, 32, FF), BF16),
            pltpu.VMEM((Y, OUT, D), BF16),
            pltpu.VMEM((Y, OWN, D), BF16),
            pltpu.VMEM((256, TOK), BF16),
            pltpu.VMEM((256, TOK), BF16),
            pltpu.VMEM((2 * TOK, 256), BF16),
            pltpu.VMEM((2 * TOK, 256), BF16),
            pltpu.VMEM((V_A, 2 * TOK), BF16),
            pltpu.VMEM((V_B, 2 * TOK), BF16),
            pltpu.VMEM((X, OUT, TOK), F32),
            pltpu.VMEM((X, 8, TOK), F32),
            pltpu.VMEM((X, OUT, TOK), BF16),
            pltpu.VMEM((X, OUT, TOK), BF16),
            pltpu.VMEM((X, 8, TOK), F32),
            pltpu.VMEM((Y, OUT, TOK), BF16),
            pltpu.VMEM((TOK, D), BF16),
            pltpu.VMEM((TOK, D), BF16),
            pltpu.VMEM((TOK, FF), BF16),
            pltpu.VMEM((4, Y, OWN, 512), BF16),
            pltpu.VMEM((Y, 4, OWN, 512), BF16),
            dma((7,)),
            dma((2, 5)),
            dma((2, 5)),
            dma((2, 5)),
            dma((2, 5)),
            dma((3,)),
            dma((3,)),
            dma((3,)),
            dma((3,)),
            dma((2, 5)),
            dma((2, 5)),
            dma((2, 5)),
            dma((2, 5)),
            dma((2, 5)),
            dma((2, 5)),
            dma((3,)),
            dma((3,)),
            dma((4,)),
            dma((4,)),
            dma((3,)),
            dma((3,)),
            dma((3,)),
            dma((3,)),
            dma((3,)),
            dma((3,)),
            dma((3,)),
            dma((3,)),
            dma((3,)),
            dma((3,)),
            dma((3,)),
            dma((3,)),
            dma((3, 4)),
            dma((3, 4)),
        ],
        compiler_params=pltpu.CompilerParams(
            collective_id=0, has_side_effects=True, vmem_limit_bytes=56 * 1024 * 1024
        ),
        name="layer",
    )(
        packed,
        queries,
        w_up,
        w_down.T,
        w_out_a,
        w_out_b,
        stream,
        wt,
        latent_gain.reshape(1, RANK),
        gains,
        norm_gain.reshape(1, D),
        trig,
    )


def solution(mesh):
    in_specs = (
        P(("sp", "tp"), None),
        P("sp", "tp"),
        P("sp", "tp"),
        P("sp", None),
        P("sp", None),
        P(),
        P(),
        P(),
        P(None, "tp"),
        P(None, "tp"),
        P(None, "tp"),
        P(None, "tp"),
        P("tp", None),
        P("tp", None),
        P(),
        P("sp", "tp"),
        P("tp", "sp"),
    )
    out_specs = P(("sp", "tp"), None)
    return jax.shard_map(body, mesh=mesh, in_specs=in_specs, out_specs=out_specs, check_vma=False)
```

time: 326 us -> 102 us (0.31); the launches traced: 320 us -> 101 us
  waiting for transfers between devices: 116 us -> 0 us
  matrix products: 95.2 us -> 0 us
  Pallas kernels: 0 us -> 91.6 us
  local copies, waits for them, and re-layouts: 40.8 us -> 5.39 us
  blocking collectives: 33.6 us -> 0 us
  between operations: 13.6 us -> 0.08 us
  other arithmetic: 15.4 us -> 4.18 us
  starting transfers between devices: 3.56 us -> 0 us
    all_gather x2 -> x0, waiting for transfers between devices: 103 us -> none  [the longest x1 103 us: sent_together(): result = lax.all_gather(both, axis, axis=dim, tiled=True)]
    dot_general x71 -> x0, matrix products: 95.2 us -> none  [the longest x32 42.6 us: attend(): jnp.einsum('qhd,khd->qhk', query_view, key_view, preferred_element_type=j...]
    pallas_call x0 -> x1, Pallas kernels: none -> 91.6 us  [body(): pl.pallas_call(kernel, out_shape=jax.ShapeDtypeStruct((OWN, D), BF16), in...]
    all_to_all x2 -> x0, blocking collectives: 33.6 us -> none  [summed_on_arrival(): blocks = lax.all_to_all(cut_along(shard, dim, size), axis, 0, 0, tiled=True)]
    unnamed x20 -> x25, local copies, waits for them, and re-layouts: 26 us -> 4.5 us
    all_to_all x1 -> x0, waiting for transfers between devices: 13.8 us -> none  [copy_for_each(): return lax.all_to_all(copies, axis, split_axis=0, concat_axis=0, tiled=True)]
    split x5 -> x0, local copies, waits for them, and re-layouts: 13.6 us -> none  [sent_together(): jnp.split(result, [sum(widths[:k]) for k in range(1, len(widths))], axis=...]
    reduce_sum x38 -> x0, other arithmetic: 10.2 us -> none  [the longest x32 7.12 us: attend(): totals = totals * factor + jnp.sum(shifted, axis=-1)]
  transfers between devices with their start and end apart: 3 -> 0, of which waited for: 2 -> 0; matrix products, arithmetic and copies ran while one was open for 42% -> 0% of each run, Pallas kernels for 0% -> 0%
where the time goes in v1:
time: 102 us; the launch traced here: 101 us
  Pallas kernels  91.6 us (90%)
  local copies, waits for them, and re-layouts  5.39 us (5%)
  other arithmetic  4.18 us (4%)
    pallas_call x1, Pallas kernels, body(): pl.pallas_call(kernel, out_shape=jax.ShapeDtypeStruct((OWN, D), BF16), in...  91.6 us
    unnamed x25, local copies, waits for them, and re-layouts  4.5 us

profile of v1, /device:TPU:1, one launch (start us, length us, event | category | flops | bytes accessed | tf_op | source)
XLA Modules:
  0.0 101.3 jit_solution(1405229743898404890)
XLA Ops:
  0.0 0.1 add_multiply_fusion
  0.1 0.1 mul.38
  0.2 0.1 add_convert_fusion
  0.3 1.0 multiply_cosine_fusion
  1.2 0.0 copy-start.2
  1.3 0.8 pad_maximum_fusion.trig
  2.1 0.0 copy-done.2
  2.1 0.0 copy-start.3
  2.1 0.1 copy.24
  2.2 0.7 copy-done.3
  2.9 0.0 copy-start.5
  2.9 0.0 copy-start.6
  2.9 0.1 copy.25
  3.1 0.6 copy-done.5
  3.7 0.0 copy-done.6
  3.7 0.0 copy-start.1
  3.7 0.7 maximum_bitcast_fusion.wt
  4.4 0.2 copy-done.1
  4.6 0.0 copy-start.4
  4.6 0.1 copy.23
  4.7 0.7 copy-done.4
  5.4 0.1 copy.22
  5.5 0.0 copy-start.8
  5.5 0.0 copy-start.9
  5.6 0.8 pad_maximum_fusion.2.q_in
  6.3 0.0 copy-done.8
  6.3 0.0 copy-done.9
  6.3 0.1 pad_maximum_fusion.3
  6.4 0.0 copy-start
  6.4 0.0 copy-start.7
  6.4 0.8 broadcast_in_dim.2.kgain
  7.2 0.1 copy-done
  7.3 0.0 copy-done.7
  7.3 0.7 pad_maximum_fusion.1.lat_in
  8.0 91.6 %layer.1 = bf16[64,2048]{1,0:T(8,128)(2,1)} custom-call(bf16[288,256]{1,0:T(8,128)(2,1)} %pad_maximum_fusion.1.lat_in, bf16[256,256]{1,0:T(8,128)(2,1)} %pad_maximum_fusion.2.q_in, bf16[32,1024]{1,0:T(8,128)(2,1)} %up_in.1, bf16[32,1024]{1,0:T(8,128)(2,1)} %bitcast.6, bf16[64,2048]{1,0:T(8,128)(2,1)} %woa_in.1, bf16[128,2048]{1,0:T(8,128)(2,1)} %wob_in.1, ...), custom_call_target="tpu_custom_call" | custom-call | tf_op jit(solution)/shard_map/layer/pallas_call | solution.py:548
  99.6 1.7 %copy.27 = bf16[64,2048]{1,0:T(8,128)(2,1)} copy(bf16[64,2048]{1,0:T(8,128)(2,1)} %layer.1) | data formatting | bytes 524288
  (2 shorter events, 0.0 us)
Async XLA Ops:
  1.2 0.8 copy-start.2
  2.1 0.8 copy-start.3
  2.9 0.8 copy-start.5
  2.9 0.8 copy-start.6
  3.7 0.9 copy-start.1
  4.6 0.8 copy-start.4
  5.5 0.8 copy-start.8
  5.5 0.8 copy-start.9
  6.4 0.9 copy-start
  6.4 0.9 copy-start.7
